TPU v7x, 256 devices: a 2x2x32 block of a 4x16x32 slice. The times are simulated.
256 devices in a mesh: grp: 4 (over y, x), ep: 32 (over z), tp: 2 (over core).
Axes of the slice: x: 2, y: 2, z: 32, core: 2. Of those that a mesh axis runs over, the one named last changes fastest.
The devices are a block of a 4x16x32 slice.
Arguments:
- tokens: bfloat16 [8192, 2048], P(('grp', 'ep')), parts along dimension 0, may hold values from -6 to 6
- norm_gain: float32 [2048], replicated, may hold values from 0.1 to 1.9
- expert_gate: bfloat16 [32, 2048, 512], P('ep', None, 'tp'), may hold values from -0.125 to 0.125
- expert_up: bfloat16 [32, 2048, 512], P('ep', None, 'tp'), may hold values from -0.125 to 0.125
- expert_down: bfloat16 [32, 512, 2048], P('ep', 'tp'), may hold values from -0.25 to 0.25
- shared_gate: bfloat16 [2048, 512], P(None, 'tp'), may hold values from -0.125 to 0.125
- shared_up: bfloat16 [2048, 512], P(None, 'tp'), may hold values from -0.125 to 0.125
- shared_down: bfloat16 [512, 2048], P('tp'), may hold values from -0.25 to 0.25
- routes: int32 [8192, 8], P(('grp', 'ep')), parts along dimension 0, may hold values from 0 to 31, all different within a row; in each aligned block of 64 rows (0 to 63, 64 to 127, ...) at most 32 rows name the same one
- route_weights: float32 [8192, 8], P(('grp', 'ep')), parts along dimension 0, may hold values from 0.05 to 0.6
Outputs:
- mixed: bfloat16 [8192, 2048], P(('grp', 'ep'), 'tp'), parts along dimension 0
There are 4 independent parts, one for each index of `grp`. A program takes and returns all parts, laid end to end along the dimension named above; an argument that names none is the same for every part. Nothing has to cross between parts.
Inputs may be any that keep to these rules, and one draw needn't show every extreme that they name: `routes`: each row names 8 different experts. Within the rows of one index of ep no expert is named more than 32 times, a bound that some block reaches by the rows of some index of ep.
All inputs are finite; a program needn't handle non-finite values.
Results may differ from a plain program's by a relative error of at most 0.0085.
Values may be sent and summed in bfloat16 or wider, within the bound.
No kernel may reach another device: no remote copies, remote signals or barrier semaphores. Data moves between devices by JAX's collectives and lax.ppermute only.
A program may use at most 64 MiB of HBM per device.

v0:
```python
import jax
import jax.numpy as jnp
from jax import lax
from jax.sharding import PartitionSpec as P

CHAINS = 1
LEAP = 8
LATE = 2
LANES = 128


def rms_scaled(values, gain):
    wide = values.astype(jnp.float32)
    scaled = wide * lax.rsqrt(jnp.mean(wide * wide, axis=-1, keepdims=True) + 1e-06)
    return (scaled * gain).astype(jnp.bfloat16)


def ring_pairs(ring, cores, step):
    pairs = []
    for place in range(ring):
        for core in cores:
            shift = step if core == 0 else -step
            pairs.append((place * 2 + core, (place + shift) % ring * 2 + core))
    return pairs


def moved(value, ring, cores, step):
    return lax.ppermute(value, ("ep", "tp"), ring_pairs(ring, cores, step))


def weight_columns(routes, route_weights, experts):
    named = routes[:, :, None] == jnp.arange(experts, dtype=jnp.int32)[None, None, :]
    table = jnp.sum(jnp.where(named, route_weights[:, :, None], jnp.float32(0.0)), axis=1)
    head = lax.reduce_precision(table, 8, 7)
    rest = table - head
    pad = jnp.zeros((table.shape[0], LANES - 2 * experts % LANES), jnp.float32)
    return jnp.concatenate([head, rest, pad], axis=1).astype(jnp.bfloat16)


def per_device(
    tokens,
    norm_gain,
    expert_gate,
    expert_up,
    expert_down,
    shared_gate,
    shared_up,
    shared_down,
    routes,
    route_weights,
):
    _, width = tokens.shape
    ring = lax.axis_size("ep")
    far = ring // 2
    own_expert = lax.axis_index("ep")
    core = lax.axis_index("tp")
    swap = [(0, 1), (1, 0)]
    half = width // 2

    normed = rms_scaled(tokens, norm_gain)
    columns = weight_columns(routes, route_weights, ring)
    payload = jnp.concatenate([normed, columns], axis=1)
    first = jnp.split(payload, CHAINS, axis=0)

    gate_proj = jnp.dot(normed, shared_gate, preferred_element_type=jnp.float32)
    up_proj = jnp.dot(normed, shared_up, preferred_element_type=jnp.float32)
    shared_hidden = (jax.nn.silu(gate_proj) * up_proj).astype(jnp.bfloat16)
    shared_part = jnp.dot(shared_hidden, shared_down, preferred_element_type=jnp.float32)
    shared_part = lax.optimization_barrier(shared_part)

    other_gate = lax.ppermute(expert_gate[0], "tp", swap)
    other_up = lax.ppermute(expert_up[0], "tp", swap)
    other_down = lax.ppermute(expert_down[0], "tp", swap)
    gate_up = jnp.concatenate([expert_gate[0], other_gate, expert_up[0], other_up], axis=1)
    down = jnp.concatenate([expert_down[0], other_down], axis=0)
    gate_up, down = lax.optimization_barrier((gate_up, down))
    hidden_width = down.shape[0]

    lane = lax.broadcasted_iota(jnp.int32, (1, columns.shape[1]), 1)
    is_own = (lane == own_expert) | (lane == own_expert + ring)

    def expert_rows(blocks):
        merged = jnp.concatenate(blocks, axis=0)
        weight = jnp.sum(
            jnp.where(is_own, merged[:, width:].astype(jnp.float32), 0.0), axis=1, keepdims=True
        )
        proj = jnp.dot(merged[:, :width], gate_up, preferred_element_type=jnp.float32)
        hidden = (jax.nn.silu(proj[:, :hidden_width]) * proj[:, hidden_width:]).astype(jnp.bfloat16)
        out = jnp.dot(hidden, down, preferred_element_type=jnp.float32)
        return jnp.split((out * weight).astype(jnp.bfloat16), len(blocks), axis=0)

    one = (core < 2).astype(jnp.bfloat16)
    both, lone = (0, 1), (1,)
    last = [one]

    def in_turn(step, *values):
        *tied, _ = lax.optimization_barrier((*values, last[0]))
        last[0] = step(*tied)
        return (last[0], *tied)

    blocks = [[None] * (far + 1) for _ in first]
    for chain, block in enumerate(first):
        blocks[chain][LEAP] = moved(block, ring, both, LEAP)
        blocks[chain][1] = moved(block, ring, both, 1)
    order = []
    near, distant = list(range(2, LEAP)), list(range(LEAP + 1, far + 1))
    while near or distant:
        order += distant[:1] + near[:1]
        near, distant = near[1:], distant[1:]
    for k in order:
        for chain in range(CHAINS):
            block, arrived = in_turn(lambda b: b * one, blocks[chain][k - 1])
            if k == LEAP + 1:
                blocks[chain][LEAP] = arrived
            blocks[chain][k] = moved(block, ring, both if k < far else lone, 1)
    for chain, block in enumerate(first):
        blocks[chain][far] = jnp.where(core == 1, blocks[chain][far], block)

    terms = [[None] * (far + 1) for _ in first]
    middle, turn = LEAP - LATE, far + 1 - LATE - 1
    early = [*range(1, middle), *range(LEAP, turn)]
    late = [*range(middle, LEAP), *range(turn, far + 1)]
    for group in (early, late):
        for chain in range(CHAINS):
            made = expert_rows([blocks[chain][k] for k in group])
            for k, term in zip(group, made):
                terms[chain][k] = term

    def added(s, t):
        return (s.astype(jnp.float32) + t.astype(jnp.float32)).astype(jnp.bfloat16)

    distant = [moved(term[far], ring, lone, -1) for term in terms]
    near = [moved(term[LEAP - 1], ring, both, -1) for term in terms]
    for i in range(1, max(far - LEAP, LEAP - 2) + 1):
        for chain, term in enumerate(terms):
            if i <= far - LEAP:
                total, *_ = in_turn(added, distant[chain], term[far - i])
                leap = LEAP if i == far - LEAP else 1
                distant[chain] = moved(total, ring, both, -leap)
            if i <= LEAP - 2:
                total, *_ = in_turn(added, near[chain], term[LEAP - 1 - i])
                near[chain] = moved(total, ring, both, -1)

    def halves(value):
        left, right = value[:, :half], value[:, half:]
        return jnp.where(core == 0, left, right), jnp.where(core == 0, right, left)

    own_terms = jnp.concatenate([term[far] for term in terms], axis=0).astype(jnp.float32)
    total = jnp.concatenate(near, axis=0).astype(jnp.float32) + shared_part
    kept, given = halves(total + jnp.where(core == 0, own_terms, 0.0))
    kept, given = lax.optimization_barrier((kept, given))
    mine, theirs = halves(jnp.concatenate(distant, axis=0))
    taken = lax.ppermute((given + theirs.astype(jnp.float32)).astype(jnp.bfloat16), "tp", swap)
    return (kept + mine.astype(jnp.float32) + taken.astype(jnp.float32)).astype(jnp.bfloat16)


def solution(mesh):
    in_specs = (
        P(("grp", "ep"), None),
        P(),
        P("ep", None, "tp"),
        P("ep", None, "tp"),
        P("ep", "tp", None),
        P(None, "tp"),
        P(None, "tp"),
        P("tp", None),
        P(("grp", "ep"), None),
        P(("grp", "ep"), None),
    )
    out_specs = P(("grp", "ep"), "tp")

    return jax.shard_map(per_device, mesh=mesh, in_specs=in_specs, out_specs=out_specs, check_vma=False)
```

profile of v0, /device:TPU:38, one launch (start us, length us, event | category | flops | bytes accessed | tf_op | source)
XLA Modules:
  0.0 206.4 jit_solution(16234251907616228270)
XLA Ops:
  3.4 15.5 %collective-permute-start.1 = (bf16[64,2176]{1,0:T(8,128)(2,1)S(1)}, bf16[64,2176]{1,0:T(8,128)(2,1)S(1)}, u32[]{:S(2)}, u32[]{:S(2)}) collective-permute-start(bf16[64,2176]{1,0:T(8,128)(2,1)S(1)} %concatenate.18), channel_id=1, source_target_pairs={{0,16},{1,49},{2,18},{3,51},{4,20},{5,53},{6,22},{7,55},{8,24},{9,... | collective-permute-start | bytes 835592 | tf_op jit(solution)/shard_map/ppermute | solution.py:28
  21.0 9.7 %collective-permute-start.16 = (bf16[2048,256]{1,0:T(8,128)(2,1)}, bf16[2048,256]{1,0:T(8,128)(2,1)}, u32[]{:S(2)}, u32[]{:S(2)}) collective-permute-start(bf16[2048,256]{1,0:T(8,128)(2,1)} %bitcast.16), channel_id=1, source_target_pairs={{0,1},{1,0},{2,3},{3,2},{4,5},{5,4},{6,7},{7,6},{8,9},{9,8},{10,11... | collective-permute-start | bytes 3145736 | tf_op jit(solution)/shard_map/ppermute | solution.py:71
  34.7 4.2 %collective-permute-start.3 = (bf16[64,2176]{1,0:T(8,128)(2,1)S(1)}, bf16[64,2176]{1,0:T(8,128)(2,1)S(1)}, u32[]{:S(2)}, u32[]{:S(2)}) collective-permute-start(bf16[64,2176]{1,0:T(8,128)(2,1)S(1)} %broadcast_multiply_fusion.13), channel_id=1, source_target_pairs={{0,2},{1,63},{2,4},{3,1},{4,6},{5,3},{6,8},{7,5},{8,10},{9,7},{10,... | collective-permute-start | bytes 835592 | tf_op jit(solution)/shard_map/ppermute | solution.py:28
  38.9 16.1 %collective-permute-done = bf16[64,2176]{1,0:T(8,128)(2,1)S(1)} collective-permute-done((bf16[64,2176]{1,0:T(8,128)(2,1)S(1)}, bf16[64,2176]{1,0:T(8,128)(2,1)S(1)}, u32[]{:S(2)}, u32[]{:S(2)}) %collective-permute-start) | collective-permute-done | bytes 278560 | tf_op jit(solution)/shard_map/ppermute | solution.py:28
  55.2 10.1 %collective-permute-done.3 = bf16[64,2176]{1,0:T(8,128)(2,1)S(1)} collective-permute-done((bf16[64,2176]{1,0:T(8,128)(2,1)S(1)}, bf16[64,2176]{1,0:T(8,128)(2,1)S(1)}, u32[]{:S(2)}, u32[]{:S(2)}) %collective-permute-start.3) | collective-permute-done | bytes 278560 | tf_op jit(solution)/shard_map/ppermute | solution.py:28
  65.5 2.8 %collective-permute-done.2 = bf16[64,2176]{1,0:T(8,128)(2,1)S(1)} collective-permute-done((bf16[64,2176]{1,0:T(8,128)(2,1)S(1)}, bf16[64,2176]{1,0:T(8,128)(2,1)S(1)}, u32[]{:S(2)}, u32[]{:S(2)}) %collective-permute-start.2) | collective-permute-done | bytes 278560 | tf_op jit(solution)/shard_map/ppermute | solution.py:28
  68.5 4.7 %collective-permute-done.5 = bf16[64,2176]{1,0:T(8,128)(2,1)S(1)} collective-permute-done((bf16[64,2176]{1,0:T(8,128)(2,1)S(1)}, bf16[64,2176]{1,0:T(8,128)(2,1)S(1)}, u32[]{:S(2)}, u32[]{:S(2)}) %collective-permute-start.5) | collective-permute-done | bytes 278560 | tf_op jit(solution)/shard_map/ppermute | solution.py:28
  73.4 2.8 %collective-permute-done.4 = bf16[64,2176]{1,0:T(8,128)(2,1)S(1)} collective-permute-done((bf16[64,2176]{1,0:T(8,128)(2,1)S(1)}, bf16[64,2176]{1,0:T(8,128)(2,1)S(1)}, u32[]{:S(2)}, u32[]{:S(2)}) %collective-permute-start.4) | collective-permute-done | bytes 278560 | tf_op jit(solution)/shard_map/ppermute | solution.py:28
  78.6 2.5 %collective-permute-done.7 = bf16[64,2176]{1,0:T(8,128)(2,1)S(1)} collective-permute-done((bf16[64,2176]{1,0:T(8,128)(2,1)S(1)}, bf16[64,2176]{1,0:T(8,128)(2,1)S(1)}, u32[]{:S(2)}, u32[]{:S(2)}) %collective-permute-start.7) | collective-permute-done | bytes 278560 | tf_op jit(solution)/shard_map/ppermute | solution.py:28
  81.3 2.8 %collective-permute-done.6 = bf16[64,2176]{1,0:T(8,128)(2,1)S(1)} collective-permute-done((bf16[64,2176]{1,0:T(8,128)(2,1)S(1)}, bf16[64,2176]{1,0:T(8,128)(2,1)S(1)}, u32[]{:S(2)}, u32[]{:S(2)}) %collective-permute-start.6) | collective-permute-done | bytes 278560 | tf_op jit(solution)/shard_map/ppermute | solution.py:28
  84.4 4.7 %collective-permute-done.9 = bf16[64,2176]{1,0:T(8,128)(2,1)S(1)} collective-permute-done((bf16[64,2176]{1,0:T(8,128)(2,1)S(1)}, bf16[64,2176]{1,0:T(8,128)(2,1)S(1)}, u32[]{:S(2)}, u32[]{:S(2)}) %collective-permute-start.9) | collective-permute-done | bytes 278560 | tf_op jit(solution)/shard_map/ppermute | solution.py:28
  89.2 2.8 %collective-permute-done.8 = bf16[64,2176]{1,0:T(8,128)(2,1)S(1)} collective-permute-done((bf16[64,2176]{1,0:T(8,128)(2,1)S(1)}, bf16[64,2176]{1,0:T(8,128)(2,1)S(1)}, u32[]{:S(2)}, u32[]{:S(2)}) %collective-permute-start.8) | collective-permute-done | bytes 278560 | tf_op jit(solution)/shard_map/ppermute | solution.py:28
  92.6 4.4 %collective-permute-done.11 = bf16[64,2176]{1,0:T(8,128)(2,1)S(1)} collective-permute-done((bf16[64,2176]{1,0:T(8,128)(2,1)S(1)}, bf16[64,2176]{1,0:T(8,128)(2,1)S(1)}, u32[]{:S(2)}, u32[]{:S(2)}) %collective-permute-start.11) | collective-permute-done | bytes 278560 | tf_op jit(solution)/shard_map/ppermute | solution.py:28
  97.1 3.0 %collective-permute-done.10 = bf16[64,2176]{1,0:T(8,128)(2,1)S(1)} collective-permute-done((bf16[64,2176]{1,0:T(8,128)(2,1)S(1)}, bf16[64,2176]{1,0:T(8,128)(2,1)S(1)}, u32[]{:S(2)}, u32[]{:S(2)}) %collective-permute-start.10) | collective-permute-done | bytes 278560 | tf_op jit(solution)/shard_map/ppermute | solution.py:28
  100.3 3.1 %fusion = f32[704,1024]{1,0:T(8,128)S(1)} fusion(bf16[2048,1024]{1,0:T(8,128)(2,1)S(1)} %pad_maximum_fusion, bf16[704,2176]{1,0:T(8,128)(2,1)S(1)} %constant_dynamic-update-slice_fusion.4), kind=kOutput, calls=%fused_computation.2 | convolution fusion | flops 2952790016 | bytes 9961472 | tf_op jit(solution)/shard_map/dot_general | solution.py:87
  105.6 2.5 %collective-permute-done.12 = bf16[64,2176]{1,0:T(8,128)(2,1)S(1)} collective-permute-done((bf16[64,2176]{1,0:T(8,128)(2,1)S(1)}, bf16[64,2176]{1,0:T(8,128)(2,1)S(1)}, u32[]{:S(2)}, u32[]{:S(2)}) %collective-permute-start.12) | collective-permute-done | bytes 278560 | tf_op jit(solution)/shard_map/ppermute | solution.py:28
  108.1 5.2 %collective-permute-done.14 = bf16[64,2176]{1,0:T(8,128)(2,1)S(1)} collective-permute-done((bf16[64,2176]{1,0:T(8,128)(2,1)S(1)}, bf16[64,2176]{1,0:T(8,128)(2,1)S(1)}, u32[]{:S(2)}, u32[]{:S(2)}) %collective-permute-start.14) | collective-permute-done | bytes 278560 | tf_op jit(solution)/shard_map/ppermute | solution.py:28
  120.0 4.2 %collective-permute-done.19 = bf16[64,2048]{1,0:T(8,128)(2,1)S(1)} collective-permute-done((bf16[64,2048]{1,0:T(8,128)(2,1)S(1)}, bf16[64,2048]{1,0:T(8,128)(2,1)S(1)}, u32[]{:S(2)}, u32[]{:S(2)}) %collective-permute-start.19) | collective-permute-done | bytes 262176 | tf_op jit(solution)/shard_map/ppermute | solution.py:28
  124.3 3.3 %collective-permute-start.21 = (bf16[64,2048]{1,0:T(8,128)(2,1)S(1)}, bf16[64,2048]{1,0:T(8,128)(2,1)S(1)}, u32[]{:S(2)}, u32[]{:S(2)}) collective-permute-start(bf16[64,2048]{1,0:T(8,128)(2,1)S(1)} %add_convert_fusion.12), channel_id=1, source_target_pairs={{0,62},{1,3},{2,0},{3,5},{4,2},{5,7},{6,4},{7,9},{8,6},{9,11},{10,... | collective-permute-start | bytes 786440 | tf_op jit(solution)/shard_map/ppermute | solution.py:28
  127.7 3.0 %collective-permute-start.24 = (bf16[64,2048]{1,0:T(8,128)(2,1)S(1)}, bf16[64,2048]{1,0:T(8,128)(2,1)S(1)}, u32[]{:S(2)}, u32[]{:S(2)}) collective-permute-start(bf16[64,2048]{1,0:T(8,128)(2,1)S(1)} %add_convert_fusion.11), channel_id=1, source_target_pairs={{0,62},{1,3},{2,0},{3,5},{4,2},{5,7},{6,4},{7,9},{8,6},{9,11},{10,... | collective-permute-start | bytes 786440 | tf_op jit(solution)/shard_map/ppermute | solution.py:28
  131.6 3.8 %collective-permute-start.23 = (bf16[64,2048]{1,0:T(8,128)(2,1)S(1)}, bf16[64,2048]{1,0:T(8,128)(2,1)S(1)}, u32[]{:S(2)}, u32[]{:S(2)}) collective-permute-start(bf16[64,2048]{1,0:T(8,128)(2,1)S(1)} %add_convert_fusion.10), channel_id=1, source_target_pairs={{0,62},{1,3},{2,0},{3,5},{4,2},{5,7},{6,4},{7,9},{8,6},{9,11},{10,... | collective-permute-start | bytes 786440 | tf_op jit(solution)/shard_map/ppermute | solution.py:28
  135.4 3.0 %collective-permute-start.26 = (bf16[64,2048]{1,0:T(8,128)(2,1)S(1)}, bf16[64,2048]{1,0:T(8,128)(2,1)S(1)}, u32[]{:S(2)}, u32[]{:S(2)}) collective-permute-start(bf16[64,2048]{1,0:T(8,128)(2,1)S(1)} %add_convert_fusion.9), channel_id=1, source_target_pairs={{0,62},{1,3},{2,0},{3,5},{4,2},{5,7},{6,4},{7,9},{8,6},{9,11},{10,... | collective-permute-start | bytes 786440 | tf_op jit(solution)/shard_map/ppermute | solution.py:28
  139.3 3.8 %collective-permute-start.25 = (bf16[64,2048]{1,0:T(8,128)(2,1)S(1)}, bf16[64,2048]{1,0:T(8,128)(2,1)S(1)}, u32[]{:S(2)}, u32[]{:S(2)}) collective-permute-start(bf16[64,2048]{1,0:T(8,128)(2,1)S(1)} %add_convert_fusion.8), channel_id=1, source_target_pairs={{0,62},{1,3},{2,0},{3,5},{4,2},{5,7},{6,4},{7,9},{8,6},{9,11},{10,... | collective-permute-start | bytes 786440 | tf_op jit(solution)/shard_map/ppermute | solution.py:28
  143.2 3.0 %collective-permute-start.28 = (bf16[64,2048]{1,0:T(8,128)(2,1)S(1)}, bf16[64,2048]{1,0:T(8,128)(2,1)S(1)}, u32[]{:S(2)}, u32[]{:S(2)}) collective-permute-start(bf16[64,2048]{1,0:T(8,128)(2,1)S(1)} %add_convert_fusion.7), channel_id=1, source_target_pairs={{0,62},{1,3},{2,0},{3,5},{4,2},{5,7},{6,4},{7,9},{8,6},{9,11},{10,... | collective-permute-start | bytes 786440 | tf_op jit(solution)/shard_map/ppermute | solution.py:28
  147.1 3.8 %collective-permute-start.27 = (bf16[64,2048]{1,0:T(8,128)(2,1)S(1)}, bf16[64,2048]{1,0:T(8,128)(2,1)S(1)}, u32[]{:S(2)}, u32[]{:S(2)}) collective-permute-start(bf16[64,2048]{1,0:T(8,128)(2,1)S(1)} %add_convert_fusion.6), channel_id=1, source_target_pairs={{0,62},{1,3},{2,0},{3,5},{4,2},{5,7},{6,4},{7,9},{8,6},{9,11},{10,... | collective-permute-start | bytes 786440 | tf_op jit(solution)/shard_map/ppermute | solution.py:28
  151.0 3.0 %collective-permute-start.30 = (bf16[64,2048]{1,0:T(8,128)(2,1)S(1)}, bf16[64,2048]{1,0:T(8,128)(2,1)S(1)}, u32[]{:S(2)}, u32[]{:S(2)}) collective-permute-start(bf16[64,2048]{1,0:T(8,128)(2,1)S(1)} %add_convert_fusion.5), channel_id=1, source_target_pairs={{0,62},{1,3},{2,0},{3,5},{4,2},{5,7},{6,4},{7,9},{8,6},{9,11},{10,... | collective-permute-start | bytes 786440 | tf_op jit(solution)/shard_map/ppermute | solution.py:28
  154.9 3.8 %collective-permute-start.29 = (bf16[64,2048]{1,0:T(8,128)(2,1)S(1)}, bf16[64,2048]{1,0:T(8,128)(2,1)S(1)}, u32[]{:S(2)}, u32[]{:S(2)}) collective-permute-start(bf16[64,2048]{1,0:T(8,128)(2,1)S(1)} %add_convert_fusion.4), channel_id=1, source_target_pairs={{0,62},{1,3},{2,0},{3,5},{4,2},{5,7},{6,4},{7,9},{8,6},{9,11},{10,... | collective-permute-start | bytes 786440 | tf_op jit(solution)/shard_map/ppermute | solution.py:28
  158.7 3.0 %collective-permute-start.32 = (bf16[64,2048]{1,0:T(8,128)(2,1)S(1)}, bf16[64,2048]{1,0:T(8,128)(2,1)S(1)}, u32[]{:S(2)}, u32[]{:S(2)}) collective-permute-start(bf16[64,2048]{1,0:T(8,128)(2,1)S(1)} %add_convert_fusion.3), channel_id=1, source_target_pairs={{0,62},{1,3},{2,0},{3,5},{4,2},{5,7},{6,4},{7,9},{8,6},{9,11},{10,... | collective-permute-start | bytes 786440 | tf_op jit(solution)/shard_map/ppermute | solution.py:28
  163.3 2.3 %collective-permute-done.32 = bf16[64,2048]{1,0:T(8,128)(2,1)S(1)} collective-permute-done((bf16[64,2048]{1,0:T(8,128)(2,1)S(1)}, bf16[64,2048]{1,0:T(8,128)(2,1)S(1)}, u32[]{:S(2)}, u32[]{:S(2)}) %collective-permute-start.32) | collective-permute-done | bytes 262176 | tf_op jit(solution)/shard_map/ppermute | solution.py:28
  166.4 3.7 %collective-permute-start.33 = (bf16[64,2048]{1,0:T(8,128)(2,1)}, bf16[64,2048]{1,0:T(8,128)(2,1)}, u32[]{:S(2)}, u32[]{:S(2)}) collective-permute-start(bf16[64,2048]{1,0:T(8,128)(2,1)} %add_convert_fusion.1), channel_id=1, source_target_pairs={{0,62},{1,3},{2,0},{3,5},{4,2},{5,7},{6,4},{7,9},{8,6},{9,11},{10,... | collective-permute-start | bytes 786440 | tf_op jit(solution)/shard_map/ppermute | solution.py:28
  175.3 7.0 %collective-permute-start.34 = (bf16[64,2048]{1,0:T(8,128)(2,1)S(1)}, bf16[64,2048]{1,0:T(8,128)(2,1)S(1)}, u32[]{:S(2)}, u32[]{:S(2)}) collective-permute-start(bf16[64,2048]{1,0:T(8,128)(2,1)S(1)} %add_convert_fusion), channel_id=1, source_target_pairs={{0,48},{1,17},{2,50},{3,19},{4,52},{5,21},{6,54},{7,23},{8,56},{9,... | collective-permute-start | bytes 786440 | tf_op jit(solution)/shard_map/ppermute | solution.py:28
  182.4 21.6 %collective-permute-done.34 = bf16[64,2048]{1,0:T(8,128)(2,1)S(1)} collective-permute-done((bf16[64,2048]{1,0:T(8,128)(2,1)S(1)}, bf16[64,2048]{1,0:T(8,128)(2,1)S(1)}, u32[]{:S(2)}, u32[]{:S(2)}) %collective-permute-start.34) | collective-permute-done | bytes 262176 | tf_op jit(solution)/shard_map/ppermute | solution.py:28
  (118 shorter events, 36.8 us)
Async XLA Ops:
  3.4 31.3 %collective-permute-start.1 = (bf16[64,2176]{1,0:T(8,128)(2,1)S(1)}, bf16[64,2176]{1,0:T(8,128)(2,1)S(1)}, u32[]{:S(2)}, u32[]{:S(2)}) collective-permute-start(bf16[64,2176]{1,0:T(8,128)(2,1)S(1)} %concatenate.18), channel_id=1, source_target_pairs={{0,16},{1,49},{2,18},{3,51},{4,20},{5,53},{6,22},{7,55},{8,24},{9,... | collective-permute-start | bytes 835592 | tf_op jit(solution)/shard_map/ppermute | solution.py:28
  18.9 36.1 %collective-permute-start = (bf16[64,2176]{1,0:T(8,128)(2,1)S(1)}, bf16[64,2176]{1,0:T(8,128)(2,1)S(1)}, u32[]{:S(2)}, u32[]{:S(2)}) collective-permute-start(bf16[64,2176]{1,0:T(8,128)(2,1)S(1)} %concatenate.18), channel_id=1, source_target_pairs={{0,2},{1,63},{2,4},{3,1},{4,6},{5,3},{6,8},{7,5},{8,10},{9,7},{10,... | collective-permute-start | bytes 835592 | tf_op jit(solution)/shard_map/ppermute | solution.py:28
  21.0 55.4 %collective-permute-start.16 = (bf16[2048,256]{1,0:T(8,128)(2,1)}, bf16[2048,256]{1,0:T(8,128)(2,1)}, u32[]{:S(2)}, u32[]{:S(2)}) collective-permute-start(bf16[2048,256]{1,0:T(8,128)(2,1)} %bitcast.16), channel_id=1, source_target_pairs={{0,1},{1,0},{2,3},{3,2},{4,5},{5,4},{6,7},{7,6},{8,9},{9,8},{10,11... | collective-permute-start | bytes 3145736 | tf_op jit(solution)/shard_map/ppermute | solution.py:71
  30.8 45.7 %collective-permute-start.17 = (bf16[2048,256]{1,0:T(8,128)(2,1)}, bf16[2048,256]{1,0:T(8,128)(2,1)}, u32[]{:S(2)}, u32[]{:S(2)}) collective-permute-start(bf16[2048,256]{1,0:T(8,128)(2,1)} %bitcast.14), channel_id=1, source_target_pairs={{0,1},{1,0},{2,3},{3,2},{4,5},{5,4},{6,7},{7,6},{8,9},{9,8},{10,11... | collective-permute-start | bytes 3145736 | tf_op jit(solution)/shard_map/ppermute | solution.py:72
  30.8 47.6 %collective-permute-start.18 = (bf16[256,2048]{1,0:T(8,128)(2,1)}, bf16[256,2048]{1,0:T(8,128)(2,1)S(1)}, u32[]{:S(2)}, u32[]{:S(2)}) collective-permute-start(bf16[256,2048]{1,0:T(8,128)(2,1)} %bitcast.12), channel_id=1, source_target_pairs={{0,1},{1,0},{2,3},{3,2},{4,5},{5,4},{6,7},{7,6},{8,9},{9,8},{10,11... | collective-permute-start | bytes 3145736 | tf_op jit(solution)/shard_map/ppermute | solution.py:73
  34.7 30.7 %collective-permute-start.3 = (bf16[64,2176]{1,0:T(8,128)(2,1)S(1)}, bf16[64,2176]{1,0:T(8,128)(2,1)S(1)}, u32[]{:S(2)}, u32[]{:S(2)}) collective-permute-start(bf16[64,2176]{1,0:T(8,128)(2,1)S(1)} %broadcast_multiply_fusion.13), channel_id=1, source_target_pairs={{0,2},{1,63},{2,4},{3,1},{4,6},{5,3},{6,8},{7,5},{8,10},{9,7},{10,... | collective-permute-start | bytes 835592 | tf_op jit(solution)/shard_map/ppermute | solution.py:28
  55.1 13.3 %collective-permute-start.2 = (bf16[64,2176]{1,0:T(8,128)(2,1)S(1)}, bf16[64,2176]{1,0:T(8,128)(2,1)S(1)}, u32[]{:S(2)}, u32[]{:S(2)}) collective-permute-start(bf16[64,2176]{1,0:T(8,128)(2,1)S(1)} %broadcast_multiply_fusion.12), channel_id=1, source_target_pairs={{0,2},{1,63},{2,4},{3,1},{4,6},{5,3},{6,8},{7,5},{8,10},{9,7},{10,... | collective-permute-start | bytes 835592 | tf_op jit(solution)/shard_map/ppermute | solution.py:28
  65.4 7.9 %collective-permute-start.5 = (bf16[64,2176]{1,0:T(8,128)(2,1)S(1)}, bf16[64,2176]{1,0:T(8,128)(2,1)S(1)}, u32[]{:S(2)}, u32[]{:S(2)}) collective-permute-start(bf16[64,2176]{1,0:T(8,128)(2,1)S(1)} %broadcast_multiply_fusion.11), channel_id=1, source_target_pairs={{0,2},{1,63},{2,4},{3,1},{4,6},{5,3},{6,8},{7,5},{8,10},{9,7},{10,... | collective-permute-start | bytes 835592 | tf_op jit(solution)/shard_map/ppermute | solution.py:28
  68.4 7.9 %collective-permute-start.4 = (bf16[64,2176]{1,0:T(8,128)(2,1)S(1)}, bf16[64,2176]{1,0:T(8,128)(2,1)S(1)}, u32[]{:S(2)}, u32[]{:S(2)}) collective-permute-start(bf16[64,2176]{1,0:T(8,128)(2,1)S(1)} %broadcast_multiply_fusion.10), channel_id=1, source_target_pairs={{0,2},{1,63},{2,4},{3,1},{4,6},{5,3},{6,8},{7,5},{8,10},{9,7},{10,... | collective-permute-start | bytes 835592 | tf_op jit(solution)/shard_map/ppermute | solution.py:28
  73.3 7.9 %collective-permute-start.7 = (bf16[64,2176]{1,0:T(8,128)(2,1)S(1)}, bf16[64,2176]{1,0:T(8,128)(2,1)S(1)}, u32[]{:S(2)}, u32[]{:S(2)}) collective-permute-start(bf16[64,2176]{1,0:T(8,128)(2,1)S(1)} %broadcast_multiply_fusion.9), channel_id=1, source_target_pairs={{0,2},{1,63},{2,4},{3,1},{4,6},{5,3},{6,8},{7,5},{8,10},{9,7},{10,... | collective-permute-start | bytes 835592 | tf_op jit(solution)/shard_map/ppermute | solution.py:28
  76.3 7.9 %collective-permute-start.6 = (bf16[64,2176]{1,0:T(8,128)(2,1)S(1)}, bf16[64,2176]{1,0:T(8,128)(2,1)S(1)}, u32[]{:S(2)}, u32[]{:S(2)}) collective-permute-start(bf16[64,2176]{1,0:T(8,128)(2,1)S(1)} %broadcast_multiply_fusion.8), channel_id=1, source_target_pairs={{0,2},{1,63},{2,4},{3,1},{4,6},{5,3},{6,8},{7,5},{8,10},{9,7},{10,... | collective-permute-start | bytes 835592 | tf_op jit(solution)/shard_map/ppermute | solution.py:28
  81.2 7.9 %collective-permute-start.9 = (bf16[64,2176]{1,0:T(8,128)(2,1)S(1)}, bf16[64,2176]{1,0:T(8,128)(2,1)S(1)}, u32[]{:S(2)}, u32[]{:S(2)}) collective-permute-start(bf16[64,2176]{1,0:T(8,128)(2,1)S(1)} %broadcast_multiply_fusion.7), channel_id=1, source_target_pairs={{0,2},{1,63},{2,4},{3,1},{4,6},{5,3},{6,8},{7,5},{8,10},{9,7},{10,... | collective-permute-start | bytes 835592 | tf_op jit(solution)/shard_map/ppermute | solution.py:28
  84.2 7.9 %collective-permute-start.8 = (bf16[64,2176]{1,0:T(8,128)(2,1)S(1)}, bf16[64,2176]{1,0:T(8,128)(2,1)S(1)}, u32[]{:S(2)}, u32[]{:S(2)}) collective-permute-start(bf16[64,2176]{1,0:T(8,128)(2,1)S(1)} %broadcast_multiply_fusion.6), channel_id=1, source_target_pairs={{0,2},{1,63},{2,4},{3,1},{4,6},{5,3},{6,8},{7,5},{8,10},{9,7},{10,... | collective-permute-start | bytes 835592 | tf_op jit(solution)/shard_map/ppermute | solution.py:28
  89.1 7.9 %collective-permute-start.11 = (bf16[64,2176]{1,0:T(8,128)(2,1)S(1)}, bf16[64,2176]{1,0:T(8,128)(2,1)S(1)}, u32[]{:S(2)}, u32[]{:S(2)}) collective-permute-start(bf16[64,2176]{1,0:T(8,128)(2,1)S(1)} %broadcast_multiply_fusion.5), channel_id=1, source_target_pairs={{0,2},{1,63},{2,4},{3,1},{4,6},{5,3},{6,8},{7,5},{8,10},{9,7},{10,... | collective-permute-start | bytes 835592 | tf_op jit(solution)/shard_map/ppermute | solution.py:28
  92.1 8.1 %collective-permute-start.10 = (bf16[64,2176]{1,0:T(8,128)(2,1)S(1)}, bf16[64,2176]{1,0:T(8,128)(2,1)S(1)}, u32[]{:S(2)}, u32[]{:S(2)}) collective-permute-start(bf16[64,2176]{1,0:T(8,128)(2,1)S(1)} %broadcast_multiply_fusion.4), channel_id=1, source_target_pairs={{0,2},{1,63},{2,4},{3,1},{4,6},{5,3},{6,8},{7,5},{8,10},{9,7},{10,... | collective-permute-start | bytes 835592 | tf_op jit(solution)/shard_map/ppermute | solution.py:28
  97.0 8.4 %collective-permute-start.13 = (bf16[64,2176]{1,0:T(8,128)(2,1)S(1)}, bf16[64,2176]{1,0:T(8,128)(2,1)S(1)}, u32[]{:S(2)}, u32[]{:S(2)}) collective-permute-start(bf16[64,2176]{1,0:T(8,128)(2,1)S(1)} %broadcast_multiply_fusion.3), channel_id=1, source_target_pairs={{0,2},{1,63},{2,4},{3,1},{4,6},{5,3},{6,8},{7,5},{8,10},{9,7},{10,... | collective-permute-start | bytes 835592 | tf_op jit(solution)/shard_map/ppermute | solution.py:28
  100.2 7.9 %collective-permute-start.12 = (bf16[64,2176]{1,0:T(8,128)(2,1)S(1)}, bf16[64,2176]{1,0:T(8,128)(2,1)S(1)}, u32[]{:S(2)}, u32[]{:S(2)}) collective-permute-start(bf16[64,2176]{1,0:T(8,128)(2,1)S(1)} %broadcast_multiply_fusion.2), channel_id=1, source_target_pairs={{0,2},{1,63},{2,4},{3,1},{4,6},{5,3},{6,8},{7,5},{8,10},{9,7},{10,... | collective-permute-start | bytes 835592 | tf_op jit(solution)/shard_map/ppermute | solution.py:28
  105.4 7.9 %collective-permute-start.14 = (bf16[64,2176]{1,0:T(8,128)(2,1)S(1)}, bf16[64,2176]{1,0:T(8,128)(2,1)S(1)}, u32[]{:S(2)}, u32[]{:S(2)}) collective-permute-start(bf16[64,2176]{1,0:T(8,128)(2,1)S(1)} %broadcast_multiply_fusion.1), channel_id=1, source_target_pairs={{0,2},{1,63},{2,4},{3,1},{4,6},{5,3},{6,8},{7,5},{8,10},{9,7},{10,... | collective-permute-start | bytes 835592 | tf_op jit(solution)/shard_map/ppermute | solution.py:28
  119.9 7.7 %collective-permute-start.22 = (bf16[64,2048]{1,0:T(8,128)(2,1)S(1)}, bf16[64,2048]{1,0:T(8,128)(2,1)S(1)}, u32[]{:S(2)}, u32[]{:S(2)}) collective-permute-start(bf16[64,2048]{1,0:T(8,128)(2,1)S(1)} %add_convert_fusion.13), channel_id=1, source_target_pairs={{0,62},{1,3},{2,0},{3,5},{4,2},{5,7},{6,4},{7,9},{8,6},{9,11},{10,... | collective-permute-start | bytes 786440 | tf_op jit(solution)/shard_map/ppermute | solution.py:28
  124.3 7.2 %collective-permute-start.21 = (bf16[64,2048]{1,0:T(8,128)(2,1)S(1)}, bf16[64,2048]{1,0:T(8,128)(2,1)S(1)}, u32[]{:S(2)}, u32[]{:S(2)}) collective-permute-start(bf16[64,2048]{1,0:T(8,128)(2,1)S(1)} %add_convert_fusion.12), channel_id=1, source_target_pairs={{0,62},{1,3},{2,0},{3,5},{4,2},{5,7},{6,4},{7,9},{8,6},{9,11},{10,... | collective-permute-start | bytes 786440 | tf_op jit(solution)/shard_map/ppermute | solution.py:28
  127.7 7.7 %collective-permute-start.24 = (bf16[64,2048]{1,0:T(8,128)(2,1)S(1)}, bf16[64,2048]{1,0:T(8,128)(2,1)S(1)}, u32[]{:S(2)}, u32[]{:S(2)}) collective-permute-start(bf16[64,2048]{1,0:T(8,128)(2,1)S(1)} %add_convert_fusion.11), channel_id=1, source_target_pairs={{0,62},{1,3},{2,0},{3,5},{4,2},{5,7},{6,4},{7,9},{8,6},{9,11},{10,... | collective-permute-start | bytes 786440 | tf_op jit(solution)/shard_map/ppermute | solution.py:28
  131.6 7.7 %collective-permute-start.23 = (bf16[64,2048]{1,0:T(8,128)(2,1)S(1)}, bf16[64,2048]{1,0:T(8,128)(2,1)S(1)}, u32[]{:S(2)}, u32[]{:S(2)}) collective-permute-start(bf16[64,2048]{1,0:T(8,128)(2,1)S(1)} %add_convert_fusion.10), channel_id=1, source_target_pairs={{0,62},{1,3},{2,0},{3,5},{4,2},{5,7},{6,4},{7,9},{8,6},{9,11},{10,... | collective-permute-start | bytes 786440 | tf_op jit(solution)/shard_map/ppermute | solution.py:28
  135.4 7.7 %collective-permute-start.26 = (bf16[64,2048]{1,0:T(8,128)(2,1)S(1)}, bf16[64,2048]{1,0:T(8,128)(2,1)S(1)}, u32[]{:S(2)}, u32[]{:S(2)}) collective-permute-start(bf16[64,2048]{1,0:T(8,128)(2,1)S(1)} %add_convert_fusion.9), channel_id=1, source_target_pairs={{0,62},{1,3},{2,0},{3,5},{4,2},{5,7},{6,4},{7,9},{8,6},{9,11},{10,... | collective-permute-start | bytes 786440 | tf_op jit(solution)/shard_map/ppermute | solution.py:28
  139.3 7.7 %collective-permute-start.25 = (bf16[64,2048]{1,0:T(8,128)(2,1)S(1)}, bf16[64,2048]{1,0:T(8,128)(2,1)S(1)}, u32[]{:S(2)}, u32[]{:S(2)}) collective-permute-start(bf16[64,2048]{1,0:T(8,128)(2,1)S(1)} %add_convert_fusion.8), channel_id=1, source_target_pairs={{0,62},{1,3},{2,0},{3,5},{4,2},{5,7},{6,4},{7,9},{8,6},{9,11},{10,... | collective-permute-start | bytes 786440 | tf_op jit(solution)/shard_map/ppermute | solution.py:28
  143.2 7.7 %collective-permute-start.28 = (bf16[64,2048]{1,0:T(8,128)(2,1)S(1)}, bf16[64,2048]{1,0:T(8,128)(2,1)S(1)}, u32[]{:S(2)}, u32[]{:S(2)}) collective-permute-start(bf16[64,2048]{1,0:T(8,128)(2,1)S(1)} %add_convert_fusion.7), channel_id=1, source_target_pairs={{0,62},{1,3},{2,0},{3,5},{4,2},{5,7},{6,4},{7,9},{8,6},{9,11},{10,... | collective-permute-start | bytes 786440 | tf_op jit(solution)/shard_map/ppermute | solution.py:28
  147.1 7.7 %collective-permute-start.27 = (bf16[64,2048]{1,0:T(8,128)(2,1)S(1)}, bf16[64,2048]{1,0:T(8,128)(2,1)S(1)}, u32[]{:S(2)}, u32[]{:S(2)}) collective-permute-start(bf16[64,2048]{1,0:T(8,128)(2,1)S(1)} %add_convert_fusion.6), channel_id=1, source_target_pairs={{0,62},{1,3},{2,0},{3,5},{4,2},{5,7},{6,4},{7,9},{8,6},{9,11},{10,... | collective-permute-start | bytes 786440 | tf_op jit(solution)/shard_map/ppermute | solution.py:28
  151.0 7.7 %collective-permute-start.30 = (bf16[64,2048]{1,0:T(8,128)(2,1)S(1)}, bf16[64,2048]{1,0:T(8,128)(2,1)S(1)}, u32[]{:S(2)}, u32[]{:S(2)}) collective-permute-start(bf16[64,2048]{1,0:T(8,128)(2,1)S(1)} %add_convert_fusion.5), channel_id=1, source_target_pairs={{0,62},{1,3},{2,0},{3,5},{4,2},{5,7},{6,4},{7,9},{8,6},{9,11},{10,... | collective-permute-start | bytes 786440 | tf_op jit(solution)/shard_map/ppermute | solution.py:28
  154.9 7.7 %collective-permute-start.29 = (bf16[64,2048]{1,0:T(8,128)(2,1)S(1)}, bf16[64,2048]{1,0:T(8,128)(2,1)S(1)}, u32[]{:S(2)}, u32[]{:S(2)}) collective-permute-start(bf16[64,2048]{1,0:T(8,128)(2,1)S(1)} %add_convert_fusion.4), channel_id=1, source_target_pairs={{0,62},{1,3},{2,0},{3,5},{4,2},{5,7},{6,4},{7,9},{8,6},{9,11},{10,... | collective-permute-start | bytes 786440 | tf_op jit(solution)/shard_map/ppermute | solution.py:28
  158.7 6.8 %collective-permute-start.32 = (bf16[64,2048]{1,0:T(8,128)(2,1)S(1)}, bf16[64,2048]{1,0:T(8,128)(2,1)S(1)}, u32[]{:S(2)}, u32[]{:S(2)}) collective-permute-start(bf16[64,2048]{1,0:T(8,128)(2,1)S(1)} %add_convert_fusion.3), channel_id=1, source_target_pairs={{0,62},{1,3},{2,0},{3,5},{4,2},{5,7},{6,4},{7,9},{8,6},{9,11},{10,... | collective-permute-start | bytes 786440 | tf_op jit(solution)/shard_map/ppermute | solution.py:28
  166.4 7.9 %collective-permute-start.33 = (bf16[64,2048]{1,0:T(8,128)(2,1)}, bf16[64,2048]{1,0:T(8,128)(2,1)}, u32[]{:S(2)}, u32[]{:S(2)}) collective-permute-start(bf16[64,2048]{1,0:T(8,128)(2,1)} %add_convert_fusion.1), channel_id=1, source_target_pairs={{0,62},{1,3},{2,0},{3,5},{4,2},{5,7},{6,4},{7,9},{8,6},{9,11},{10,... | collective-permute-start | bytes 786440 | tf_op jit(solution)/shard_map/ppermute | solution.py:28
  172.1 10.2 %collective-permute-start.31 = (bf16[64,2048]{1,0:T(8,128)(2,1)}, bf16[64,2048]{1,0:T(8,128)(2,1)S(1)}, u32[]{:S(2)}, u32[]{:S(2)}) collective-permute-start(bf16[64,2048]{1,0:T(8,128)(2,1)} %add_convert_fusion.2), channel_id=1, source_target_pairs={{0,62},{1,3},{2,0},{3,5},{4,2},{5,7},{6,4},{7,9},{8,6},{9,11},{10,... | collective-permute-start | bytes 786440 | tf_op jit(solution)/shard_map/ppermute | solution.py:28
  175.3 28.7 %collective-permute-start.34 = (bf16[64,2048]{1,0:T(8,128)(2,1)S(1)}, bf16[64,2048]{1,0:T(8,128)(2,1)S(1)}, u32[]{:S(2)}, u32[]{:S(2)}) collective-permute-start(bf16[64,2048]{1,0:T(8,128)(2,1)S(1)} %add_convert_fusion), channel_id=1, source_target_pairs={{0,48},{1,17},{2,50},{3,19},{4,52},{5,21},{6,54},{7,23},{8,56},{9,... | collective-permute-start | bytes 786440 | tf_op jit(solution)/shard_map/ppermute | solution.py:28
  (8 other events, 274.2 us)
where the time goes:
time: 208 us; the launch traced here: 206 us
  waiting for transfers between devices  102 us (49%)
  starting transfers between devices  82.2 us (40%)
  matrix products  11 us (5%)
  other arithmetic  10.1 us (5%)
    ppermute x32, waiting for transfers between devices, moved(): return lax.ppermute(value, ('ep', 'tp'), ring_pairs(ring, cores, step))  101 us
    ppermute x32, starting transfers between devices, moved(): return lax.ppermute(value, ('ep', 'tp'), ring_pairs(ring, cores, step))  71.3 us
    ppermute x1, starting transfers between devices, per_device(): other_gate = lax.ppermute(expert_gate[0], 'tp', swap)  9.75 us
    dot_general x2, matrix products, expert_rows(): jnp.dot(merged[:, :width], gate_up, preferred_element_type=jnp.float32)  4.65 us
  transfers between devices with their start and end apart: 36, of which 24 were waited for; matrix products, arithmetic and copies ran while one was open for 7% of the time, Pallas kernels for 0%

commit v1 on v0

--- a/solution.py
+++ b/solution.py
@@ -15,17 +15,25 @@
     return (scaled * gain).astype(jnp.bfloat16)
 
 
-def ring_pairs(ring, cores, step):
+def ring_pairs(ring, flows, places, change, back):
+    before, after = change
     pairs = []
     for place in range(ring):
-        for core in cores:
-            shift = step if core == 0 else -step
-            pairs.append((place * 2 + core, (place + shift) % ring * 2 + core))
+        for flow in flows:
+            shift = places if flow == 0 else -places
+            source = place * 2 + (before ^ flow)
+            target = (place + shift) % ring * 2 + (after ^ flow)
+            pairs.append((target, source) if back else (source, target))
     return pairs
 
 
-def moved(value, ring, cores, step):
-    return lax.ppermute(value, ("ep", "tp"), ring_pairs(ring, cores, step))
+def moved(value, ring, flows, k, back=False):
+    if k == LEAP:
+        pairs = ring_pairs(ring, flows, LEAP, (0, 0), back)
+    else:
+        on = (k if k < LEAP else k - LEAP) % 2
+        pairs = ring_pairs(ring, flows, 1, (1 - on, on), back)
+    return lax.ppermute(value, ("ep", "tp"), pairs)
 
 
 def weight_columns(routes, route_weights, experts):
@@ -112,7 +120,7 @@
             block, arrived = in_turn(lambda b: b * one, blocks[chain][k - 1])
             if k == LEAP + 1:
                 blocks[chain][LEAP] = arrived
-            blocks[chain][k] = moved(block, ring, both if k < far else lone, 1)
+            blocks[chain][k] = moved(block, ring, both if k < far else lone, k)
     for chain, block in enumerate(first):
         blocks[chain][far] = jnp.where(core == 1, blocks[chain][far], block)
 
@@ -129,17 +137,16 @@
     def added(s, t):
         return (s.astype(jnp.float32) + t.astype(jnp.float32)).astype(jnp.bfloat16)
 
-    distant = [moved(term[far], ring, lone, -1) for term in terms]
-    near = [moved(term[LEAP - 1], ring, both, -1) for term in terms]
+    distant = [moved(term[far], ring, lone, far, back=True) for term in terms]
+    near = [moved(term[LEAP - 1], ring, both, LEAP - 1, back=True) for term in terms]
     for i in range(1, max(far - LEAP, LEAP - 2) + 1):
         for chain, term in enumerate(terms):
             if i <= far - LEAP:
                 total, *_ = in_turn(added, distant[chain], term[far - i])
-                leap = LEAP if i == far - LEAP else 1
-                distant[chain] = moved(total, ring, both, -leap)
+                distant[chain] = moved(total, ring, both, far - i, back=True)
             if i <= LEAP - 2:
                 total, *_ = in_turn(added, near[chain], term[LEAP - 1 - i])
-                near[chain] = moved(total, ring, both, -1)
+                near[chain] = moved(total, ring, both, LEAP - 1 - i, back=True)
 
     def halves(value):
         left, right = value[:, :half], value[:, half:]

time: 208 us -> 239 us (1.15)
  starting transfers between devices: 82.2 us -> 120 us
  waiting for transfers between devices: 102 us -> 95.2 us
    ppermute x32, starting transfers between devices: 71.3 us -> 104 us  [moved(): return lax.ppermute(value, ('ep', 'tp'), pairs)]
    ppermute x1, starting transfers between devices: 0.6 us -> 15.7 us  [per_device(): lax.ppermute((given + theirs.astype(jnp.float32)).astype(jnp.bfloat16), '...]
    ppermute x1, starting transfers between devices: 9.75 us -> 0.01 us  [per_device(): other_gate = lax.ppermute(expert_gate[0], 'tp', swap)]
    ppermute x32, waiting for transfers between devices: 101 us -> 94.2 us  [moved(): return lax.ppermute(value, ('ep', 'tp'), pairs)]
  transfers between devices with their start and end apart: 36 -> 36, of which waited for: 24 -> 24; matrix products, arithmetic and copies ran while one was open for 7% -> 6% of each run, Pallas kernels for 0% -> 0%
where the time goes in v1:
time: 239 us; the launch traced here: 238 us
  starting transfers between devices  120 us (50%)
  waiting for transfers between devices  95.2 us (40%)
  matrix products  11 us (5%)
  other arithmetic  10.1 us (4%)
    ppermute x32, starting transfers between devices, moved(): return lax.ppermute(value, ('ep', 'tp'), pairs)  104 us
    ppermute x32, waiting for transfers between devices, moved(): return lax.ppermute(value, ('ep', 'tp'), pairs)  94.2 us
    ppermute x1, starting transfers between devices, per_device(): lax.ppermute((given + theirs.astype(jnp.float32)).astype(jnp.bfloat16), '...  15.7 us
  transfers between devices with their start and end apart: 36, of which 24 were waited for; matrix products, arithmetic and copies ran while one was open for 6% of the time, Pallas kernels for 0%

profile of v1, /device:TPU:38, one launch (start us, length us, event | category | flops | bytes accessed | tf_op | source)
XLA Modules:
  0.0 237.8 jit_solution(1761762872280948519)
XLA Ops:
  3.4 15.5 %collective-permute-start.1 = (bf16[64,2176]{1,0:T(8,128)(2,1)S(1)}, bf16[64,2176]{1,0:T(8,128)(2,1)S(1)}, u32[]{:S(2)}, u32[]{:S(2)}) collective-permute-start(bf16[64,2176]{1,0:T(8,128)(2,1)S(1)} %concatenate.18), channel_id=1, source_target_pairs={{0,16},{1,49},{2,18},{3,51},{4,20},{5,53},{6,22},{7,55},{8,24},{9,... | collective-permute-start | bytes 835592 | tf_op jit(solution)/shard_map/ppermute | solution.py:36
  18.9 11.0 %collective-permute-start = (bf16[64,2176]{1,0:T(8,128)(2,1)S(1)}, bf16[64,2176]{1,0:T(8,128)(2,1)S(1)}, u32[]{:S(2)}, u32[]{:S(2)}) collective-permute-start(bf16[64,2176]{1,0:T(8,128)(2,1)S(1)} %concatenate.18), channel_id=1, source_target_pairs={{0,3},{1,62},{2,5},{3,0},{4,7},{5,2},{6,9},{7,4},{8,11},{9,6},{10,... | collective-permute-start | bytes 835592 | tf_op jit(solution)/shard_map/ppermute | solution.py:36
  34.7 18.5 %collective-permute-start.3 = (bf16[64,2176]{1,0:T(8,128)(2,1)S(1)}, bf16[64,2176]{1,0:T(8,128)(2,1)S(1)}, u32[]{:S(2)}, u32[]{:S(2)}) collective-permute-start(bf16[64,2176]{1,0:T(8,128)(2,1)S(1)} %broadcast_multiply_fusion.13), channel_id=1, source_target_pairs={{0,3},{1,62},{2,5},{3,0},{4,7},{5,2},{6,9},{7,4},{8,11},{9,6},{10,... | collective-permute-start | bytes 835592 | tf_op jit(solution)/shard_map/ppermute | solution.py:36
  53.2 3.6 %collective-permute-done = bf16[64,2176]{1,0:T(8,128)(2,1)S(1)} collective-permute-done((bf16[64,2176]{1,0:T(8,128)(2,1)S(1)}, bf16[64,2176]{1,0:T(8,128)(2,1)S(1)}, u32[]{:S(2)}, u32[]{:S(2)}) %collective-permute-start) | collective-permute-done | bytes 278560 | tf_op jit(solution)/shard_map/ppermute | solution.py:36
  56.8 3.6 %collective-permute-start.2 = (bf16[64,2176]{1,0:T(8,128)(2,1)S(1)}, bf16[64,2176]{1,0:T(8,128)(2,1)S(1)}, u32[]{:S(2)}, u32[]{:S(2)}) collective-permute-start(bf16[64,2176]{1,0:T(8,128)(2,1)S(1)} %broadcast_multiply_fusion.12), channel_id=1, source_target_pairs={{1,2},{0,63},{3,4},{2,1},{5,6},{4,3},{7,8},{6,5},{9,10},{8,7},{11,... | collective-permute-start | bytes 835592 | tf_op jit(solution)/shard_map/ppermute | solution.py:36
  60.5 5.5 %collective-permute-start.5 = (bf16[64,2176]{1,0:T(8,128)(2,1)S(1)}, bf16[64,2176]{1,0:T(8,128)(2,1)S(1)}, u32[]{:S(2)}, u32[]{:S(2)}) collective-permute-start(bf16[64,2176]{1,0:T(8,128)(2,1)S(1)} %broadcast_multiply_fusion.11), channel_id=1, source_target_pairs={{1,2},{0,63},{3,4},{2,1},{5,6},{4,3},{7,8},{6,5},{9,10},{8,7},{11,... | collective-permute-start | bytes 835592 | tf_op jit(solution)/shard_map/ppermute | solution.py:36
  67.6 3.1 %collective-permute-done.5 = bf16[64,2176]{1,0:T(8,128)(2,1)S(1)} collective-permute-done((bf16[64,2176]{1,0:T(8,128)(2,1)S(1)}, bf16[64,2176]{1,0:T(8,128)(2,1)S(1)}, u32[]{:S(2)}, u32[]{:S(2)}) %collective-permute-start.5) | collective-permute-done | bytes 278560 | tf_op jit(solution)/shard_map/ppermute | solution.py:36
  70.9 4.6 %collective-permute-done.4 = bf16[64,2176]{1,0:T(8,128)(2,1)S(1)} collective-permute-done((bf16[64,2176]{1,0:T(8,128)(2,1)S(1)}, bf16[64,2176]{1,0:T(8,128)(2,1)S(1)}, u32[]{:S(2)}, u32[]{:S(2)}) %collective-permute-start.4) | collective-permute-done | bytes 278560 | tf_op jit(solution)/shard_map/ppermute | solution.py:36
  75.5 4.1 %collective-permute-start.6 = (bf16[64,2176]{1,0:T(8,128)(2,1)S(1)}, bf16[64,2176]{1,0:T(8,128)(2,1)S(1)}, u32[]{:S(2)}, u32[]{:S(2)}) collective-permute-start(bf16[64,2176]{1,0:T(8,128)(2,1)S(1)} %broadcast_multiply_fusion.8), channel_id=1, source_target_pairs={{1,2},{0,63},{3,4},{2,1},{5,6},{4,3},{7,8},{6,5},{9,10},{8,7},{11,... | collective-permute-start | bytes 835592 | tf_op jit(solution)/shard_map/ppermute | solution.py:36
  82.5 3.8 %collective-permute-done.6 = bf16[64,2176]{1,0:T(8,128)(2,1)S(1)} collective-permute-done((bf16[64,2176]{1,0:T(8,128)(2,1)S(1)}, bf16[64,2176]{1,0:T(8,128)(2,1)S(1)}, u32[]{:S(2)}, u32[]{:S(2)}) %collective-permute-start.6) | collective-permute-done | bytes 278560 | tf_op jit(solution)/shard_map/ppermute | solution.py:36
  86.5 3.2 %collective-permute-done.9 = bf16[64,2176]{1,0:T(8,128)(2,1)S(1)} collective-permute-done((bf16[64,2176]{1,0:T(8,128)(2,1)S(1)}, bf16[64,2176]{1,0:T(8,128)(2,1)S(1)}, u32[]{:S(2)}, u32[]{:S(2)}) %collective-permute-start.9) | collective-permute-done | bytes 278560 | tf_op jit(solution)/shard_map/ppermute | solution.py:36
  89.9 4.1 %collective-permute-done.8 = bf16[64,2176]{1,0:T(8,128)(2,1)S(1)} collective-permute-done((bf16[64,2176]{1,0:T(8,128)(2,1)S(1)}, bf16[64,2176]{1,0:T(8,128)(2,1)S(1)}, u32[]{:S(2)}, u32[]{:S(2)}) %collective-permute-start.8) | collective-permute-done | bytes 278560 | tf_op jit(solution)/shard_map/ppermute | solution.py:36
  94.0 4.3 %collective-permute-start.10 = (bf16[64,2176]{1,0:T(8,128)(2,1)S(1)}, bf16[64,2176]{1,0:T(8,128)(2,1)S(1)}, u32[]{:S(2)}, u32[]{:S(2)}) collective-permute-start(bf16[64,2176]{1,0:T(8,128)(2,1)S(1)} %broadcast_multiply_fusion.4), channel_id=1, source_target_pairs={{1,2},{0,63},{3,4},{2,1},{5,6},{4,3},{7,8},{6,5},{9,10},{8,7},{11,... | collective-permute-start | bytes 835592 | tf_op jit(solution)/shard_map/ppermute | solution.py:36
  101.4 3.8 %collective-permute-done.10 = bf16[64,2176]{1,0:T(8,128)(2,1)S(1)} collective-permute-done((bf16[64,2176]{1,0:T(8,128)(2,1)S(1)}, bf16[64,2176]{1,0:T(8,128)(2,1)S(1)}, u32[]{:S(2)}, u32[]{:S(2)}) %collective-permute-start.10) | collective-permute-done | bytes 278560 | tf_op jit(solution)/shard_map/ppermute | solution.py:36
  105.5 3.1 %fusion = f32[704,1024]{1,0:T(8,128)S(1)} fusion(bf16[2048,1024]{1,0:T(8,128)(2,1)S(1)} %pad_maximum_fusion, bf16[704,2176]{1,0:T(8,128)(2,1)S(1)} %constant_dynamic-update-slice_fusion.4), kind=kOutput, calls=%fused_computation.2 | convolution fusion | flops 2952790016 | bytes 9961472 | tf_op jit(solution)/shard_map/dot_general | solution.py:95
  112.5 4.9 %collective-permute-done.14 = bf16[64,2176]{1,0:T(8,128)(2,1)S(1)} collective-permute-done((bf16[64,2176]{1,0:T(8,128)(2,1)S(1)}, bf16[64,2176]{1,0:T(8,128)(2,1)S(1)}, u32[]{:S(2)}, u32[]{:S(2)}) %collective-permute-start.14) | collective-permute-done | bytes 278560 | tf_op jit(solution)/shard_map/ppermute | solution.py:36
  117.4 4.6 %collective-permute-start.15 = (bf16[64,2176]{1,0:T(8,128)(2,1)S(1)}, bf16[64,2176]{1,0:T(8,128)(2,1)S(1)}, u32[]{:S(2)}, u32[]{:S(2)}) collective-permute-start(bf16[64,2176]{1,0:T(8,128)(2,1)S(1)} %broadcast_multiply_fusion), channel_id=1, source_target_pairs={{0,63},{2,1},{4,3},{6,5},{8,7},{10,9},{12,11},{14,13},{16,15},{18,... | collective-permute-start | bytes 835592 | tf_op jit(solution)/shard_map/ppermute | solution.py:36
  122.1 4.0 %collective-permute-done.15 = bf16[64,2176]{1,0:T(8,128)(2,1)S(1)} collective-permute-done((bf16[64,2176]{1,0:T(8,128)(2,1)S(1)}, bf16[64,2176]{1,0:T(8,128)(2,1)S(1)}, u32[]{:S(2)}, u32[]{:S(2)}) %collective-permute-start.15) | collective-permute-done | bytes 278560 | tf_op jit(solution)/shard_map/ppermute | solution.py:36
  131.5 6.2 %collective-permute-done.20 = bf16[64,2048]{1,0:T(8,128)(2,1)S(1)} collective-permute-done((bf16[64,2048]{1,0:T(8,128)(2,1)S(1)}, bf16[64,2048]{1,0:T(8,128)(2,1)S(1)}, u32[]{:S(2)}, u32[]{:S(2)}) %collective-permute-start.20) | collective-permute-done | bytes 262176 | tf_op jit(solution)/shard_map/ppermute | solution.py:36
  138.0 4.9 %collective-permute-start.21 = (bf16[64,2048]{1,0:T(8,128)(2,1)S(1)}, bf16[64,2048]{1,0:T(8,128)(2,1)S(1)}, u32[]{:S(2)}, u32[]{:S(2)}) collective-permute-start(bf16[64,2048]{1,0:T(8,128)(2,1)S(1)} %add_convert_fusion.12), channel_id=1, source_target_pairs={{2,1},{63,0},{4,3},{1,2},{6,5},{3,4},{8,7},{5,6},{10,9},{7,8},{12,... | collective-permute-start | bytes 786440 | tf_op jit(solution)/shard_map/ppermute | solution.py:36
  145.6 3.8 %collective-permute-done.21 = bf16[64,2048]{1,0:T(8,128)(2,1)S(1)} collective-permute-done((bf16[64,2048]{1,0:T(8,128)(2,1)S(1)}, bf16[64,2048]{1,0:T(8,128)(2,1)S(1)}, u32[]{:S(2)}, u32[]{:S(2)}) %collective-permute-start.21) | collective-permute-done | bytes 262176 | tf_op jit(solution)/shard_map/ppermute | solution.py:36
  149.6 3.1 %collective-permute-done.24 = bf16[64,2048]{1,0:T(8,128)(2,1)S(1)} collective-permute-done((bf16[64,2048]{1,0:T(8,128)(2,1)S(1)}, bf16[64,2048]{1,0:T(8,128)(2,1)S(1)}, u32[]{:S(2)}, u32[]{:S(2)}) %collective-permute-start.24) | collective-permute-done | bytes 262176 | tf_op jit(solution)/shard_map/ppermute | solution.py:36
  152.9 3.9 %collective-permute-done.23 = bf16[64,2048]{1,0:T(8,128)(2,1)S(1)} collective-permute-done((bf16[64,2048]{1,0:T(8,128)(2,1)S(1)}, bf16[64,2048]{1,0:T(8,128)(2,1)S(1)}, u32[]{:S(2)}, u32[]{:S(2)}) %collective-permute-start.23) | collective-permute-done | bytes 262176 | tf_op jit(solution)/shard_map/ppermute | solution.py:36
  156.9 4.3 %collective-permute-start.25 = (bf16[64,2048]{1,0:T(8,128)(2,1)S(1)}, bf16[64,2048]{1,0:T(8,128)(2,1)S(1)}, u32[]{:S(2)}, u32[]{:S(2)}) collective-permute-start(bf16[64,2048]{1,0:T(8,128)(2,1)S(1)} %add_convert_fusion.8), channel_id=1, source_target_pairs={{2,1},{63,0},{4,3},{1,2},{6,5},{3,4},{8,7},{5,6},{10,9},{7,8},{12,... | collective-permute-start | bytes 786440 | tf_op jit(solution)/shard_map/ppermute | solution.py:36
  164.0 3.6 %collective-permute-done.25 = bf16[64,2048]{1,0:T(8,128)(2,1)S(1)} collective-permute-done((bf16[64,2048]{1,0:T(8,128)(2,1)S(1)}, bf16[64,2048]{1,0:T(8,128)(2,1)S(1)}, u32[]{:S(2)}, u32[]{:S(2)}) %collective-permute-start.25) | collective-permute-done | bytes 262176 | tf_op jit(solution)/shard_map/ppermute | solution.py:36
  171.1 3.2 %collective-permute-done.27 = bf16[64,2048]{1,0:T(8,128)(2,1)S(1)} collective-permute-done((bf16[64,2048]{1,0:T(8,128)(2,1)S(1)}, bf16[64,2048]{1,0:T(8,128)(2,1)S(1)}, u32[]{:S(2)}, u32[]{:S(2)}) %collective-permute-start.27) | collective-permute-done | bytes 262176 | tf_op jit(solution)/shard_map/ppermute | solution.py:36
  174.4 5.0 %collective-permute-start.29 = (bf16[64,2048]{1,0:T(8,128)(2,1)S(1)}, bf16[64,2048]{1,0:T(8,128)(2,1)S(1)}, u32[]{:S(2)}, u32[]{:S(2)}) collective-permute-start(bf16[64,2048]{1,0:T(8,128)(2,1)S(1)} %add_convert_fusion.4), channel_id=1, source_target_pairs={{2,1},{63,0},{4,3},{1,2},{6,5},{3,4},{8,7},{5,6},{10,9},{7,8},{12,... | collective-permute-start | bytes 786440 | tf_op jit(solution)/shard_map/ppermute | solution.py:36
  182.2 3.4 %collective-permute-done.29 = bf16[64,2048]{1,0:T(8,128)(2,1)S(1)} collective-permute-done((bf16[64,2048]{1,0:T(8,128)(2,1)S(1)}, bf16[64,2048]{1,0:T(8,128)(2,1)S(1)}, u32[]{:S(2)}, u32[]{:S(2)}) %collective-permute-start.29) | collective-permute-done | bytes 262176 | tf_op jit(solution)/shard_map/ppermute | solution.py:36
  193.9 4.3 %collective-permute-done.33 = bf16[64,2048]{1,0:T(8,128)(2,1)} collective-permute-done((bf16[64,2048]{1,0:T(8,128)(2,1)}, bf16[64,2048]{1,0:T(8,128)(2,1)}, u32[]{:S(2)}, u32[]{:S(2)}) %collective-permute-start.33) | collective-permute-done | bytes 262176 | tf_op jit(solution)/shard_map/ppermute | solution.py:36
  199.2 3.5 %collective-permute-start.34 = (bf16[64,2048]{1,0:T(8,128)(2,1)S(1)}, bf16[64,2048]{1,0:T(8,128)(2,1)S(1)}, u32[]{:S(2)}, u32[]{:S(2)}) collective-permute-start(bf16[64,2048]{1,0:T(8,128)(2,1)S(1)} %add_convert_fusion), channel_id=1, source_target_pairs={{16,0},{49,1},{18,2},{51,3},{20,4},{53,5},{22,6},{55,7},{24,8},{57... | collective-permute-start | bytes 786440 | tf_op jit(solution)/shard_map/ppermute | solution.py:36
  202.9 17.4 %collective-permute-done.34 = bf16[64,2048]{1,0:T(8,128)(2,1)S(1)} collective-permute-done((bf16[64,2048]{1,0:T(8,128)(2,1)S(1)}, bf16[64,2048]{1,0:T(8,128)(2,1)S(1)}, u32[]{:S(2)}, u32[]{:S(2)}) %collective-permute-start.34) | collective-permute-done | bytes 262176 | tf_op jit(solution)/shard_map/ppermute | solution.py:36
  220.4 15.7 %collective-permute-start.35 = (bf16[64,1024]{1,0:T(8,128)(2,1)S(1)}, bf16[64,1024]{1,0:T(8,128)(2,1)S(1)}, u32[]{:S(2)}, u32[]{:S(2)}) collective-permute-start(bf16[64,1024]{1,0:T(8,128)(2,1)S(1)} %add_convert_fusion.15), channel_id=1, source_target_pairs={{0,1},{1,0},{2,3},{3,2},{4,5},{5,4},{6,7},{7,6},{8,9},{9,8},{10,11... | collective-permute-start | bytes 393224 | tf_op jit(solution)/shard_map/ppermute | solution.py:160
  (118 shorter events, 49.6 us)
Async XLA Ops:
  3.4 31.3 %collective-permute-start.1 = (bf16[64,2176]{1,0:T(8,128)(2,1)S(1)}, bf16[64,2176]{1,0:T(8,128)(2,1)S(1)}, u32[]{:S(2)}, u32[]{:S(2)}) collective-permute-start(bf16[64,2176]{1,0:T(8,128)(2,1)S(1)} %concatenate.18), channel_id=1, source_target_pairs={{0,16},{1,49},{2,18},{3,51},{4,20},{5,53},{6,22},{7,55},{8,24},{9,... | collective-permute-start | bytes 835592 | tf_op jit(solution)/shard_map/ppermute | solution.py:36
  18.9 37.9 %collective-permute-start = (bf16[64,2176]{1,0:T(8,128)(2,1)S(1)}, bf16[64,2176]{1,0:T(8,128)(2,1)S(1)}, u32[]{:S(2)}, u32[]{:S(2)}) collective-permute-start(bf16[64,2176]{1,0:T(8,128)(2,1)S(1)} %concatenate.18), channel_id=1, source_target_pairs={{0,3},{1,62},{2,5},{3,0},{4,7},{5,2},{6,9},{7,4},{8,11},{9,6},{10,... | collective-permute-start | bytes 835592 | tf_op jit(solution)/shard_map/ppermute | solution.py:36
  29.9 49.7 %collective-permute-start.16 = (bf16[2048,256]{1,0:T(8,128)(2,1)}, bf16[2048,256]{1,0:T(8,128)(2,1)}, u32[]{:S(2)}, u32[]{:S(2)}) collective-permute-start(bf16[2048,256]{1,0:T(8,128)(2,1)} %bitcast.16), channel_id=1, source_target_pairs={{0,1},{1,0},{2,3},{3,2},{4,5},{5,4},{6,7},{7,6},{8,9},{9,8},{10,11... | collective-permute-start | bytes 3145736 | tf_op jit(solution)/shard_map/ppermute | solution.py:79
  29.9 49.7 %collective-permute-start.17 = (bf16[2048,256]{1,0:T(8,128)(2,1)}, bf16[2048,256]{1,0:T(8,128)(2,1)}, u32[]{:S(2)}, u32[]{:S(2)}) collective-permute-start(bf16[2048,256]{1,0:T(8,128)(2,1)} %bitcast.14), channel_id=1, source_target_pairs={{0,1},{1,0},{2,3},{3,2},{4,5},{5,4},{6,7},{7,6},{8,9},{9,8},{10,11... | collective-permute-start | bytes 3145736 | tf_op jit(solution)/shard_map/ppermute | solution.py:80
  30.4 51.2 %collective-permute-start.18 = (bf16[256,2048]{1,0:T(8,128)(2,1)}, bf16[256,2048]{1,0:T(8,128)(2,1)S(1)}, u32[]{:S(2)}, u32[]{:S(2)}) collective-permute-start(bf16[256,2048]{1,0:T(8,128)(2,1)} %bitcast.12), channel_id=1, source_target_pairs={{0,1},{1,0},{2,3},{3,2},{4,5},{5,4},{6,7},{7,6},{8,9},{9,8},{10,11... | collective-permute-start | bytes 3145736 | tf_op jit(solution)/shard_map/ppermute | solution.py:81
  34.7 25.8 %collective-permute-start.3 = (bf16[64,2176]{1,0:T(8,128)(2,1)S(1)}, bf16[64,2176]{1,0:T(8,128)(2,1)S(1)}, u32[]{:S(2)}, u32[]{:S(2)}) collective-permute-start(bf16[64,2176]{1,0:T(8,128)(2,1)S(1)} %broadcast_multiply_fusion.13), channel_id=1, source_target_pairs={{0,3},{1,62},{2,5},{3,0},{4,7},{5,2},{6,9},{7,4},{8,11},{9,6},{10,... | collective-permute-start | bytes 835592 | tf_op jit(solution)/shard_map/ppermute | solution.py:36
  56.8 10.5 %collective-permute-start.2 = (bf16[64,2176]{1,0:T(8,128)(2,1)S(1)}, bf16[64,2176]{1,0:T(8,128)(2,1)S(1)}, u32[]{:S(2)}, u32[]{:S(2)}) collective-permute-start(bf16[64,2176]{1,0:T(8,128)(2,1)S(1)} %broadcast_multiply_fusion.12), channel_id=1, source_target_pairs={{1,2},{0,63},{3,4},{2,1},{5,6},{4,3},{7,8},{6,5},{9,10},{8,7},{11,... | collective-permute-start | bytes 835592 | tf_op jit(solution)/shard_map/ppermute | solution.py:36
  60.5 10.1 %collective-permute-start.5 = (bf16[64,2176]{1,0:T(8,128)(2,1)S(1)}, bf16[64,2176]{1,0:T(8,128)(2,1)S(1)}, u32[]{:S(2)}, u32[]{:S(2)}) collective-permute-start(bf16[64,2176]{1,0:T(8,128)(2,1)S(1)} %broadcast_multiply_fusion.11), channel_id=1, source_target_pairs={{1,2},{0,63},{3,4},{2,1},{5,6},{4,3},{7,8},{6,5},{9,10},{8,7},{11,... | collective-permute-start | bytes 835592 | tf_op jit(solution)/shard_map/ppermute | solution.py:36
  67.4 8.1 %collective-permute-start.4 = (bf16[64,2176]{1,0:T(8,128)(2,1)S(1)}, bf16[64,2176]{1,0:T(8,128)(2,1)S(1)}, u32[]{:S(2)}, u32[]{:S(2)}) collective-permute-start(bf16[64,2176]{1,0:T(8,128)(2,1)S(1)} %broadcast_multiply_fusion.10), channel_id=1, source_target_pairs={{0,3},{1,62},{2,5},{3,0},{4,7},{5,2},{6,9},{7,4},{8,11},{9,6},{10,... | collective-permute-start | bytes 835592 | tf_op jit(solution)/shard_map/ppermute | solution.py:36
  70.7 11.0 %collective-permute-start.7 = (bf16[64,2176]{1,0:T(8,128)(2,1)S(1)}, bf16[64,2176]{1,0:T(8,128)(2,1)S(1)}, u32[]{:S(2)}, u32[]{:S(2)}) collective-permute-start(bf16[64,2176]{1,0:T(8,128)(2,1)S(1)} %broadcast_multiply_fusion.9), channel_id=1, source_target_pairs={{0,3},{1,62},{2,5},{3,0},{4,7},{5,2},{6,9},{7,4},{8,11},{9,6},{10,... | collective-permute-start | bytes 835592 | tf_op jit(solution)/shard_map/ppermute | solution.py:36
  75.5 10.8 %collective-permute-start.6 = (bf16[64,2176]{1,0:T(8,128)(2,1)S(1)}, bf16[64,2176]{1,0:T(8,128)(2,1)S(1)}, u32[]{:S(2)}, u32[]{:S(2)}) collective-permute-start(bf16[64,2176]{1,0:T(8,128)(2,1)S(1)} %broadcast_multiply_fusion.8), channel_id=1, source_target_pairs={{1,2},{0,63},{3,4},{2,1},{5,6},{4,3},{7,8},{6,5},{9,10},{8,7},{11,... | collective-permute-start | bytes 835592 | tf_op jit(solution)/shard_map/ppermute | solution.py:36
  81.8 7.9 %collective-permute-start.9 = (bf16[64,2176]{1,0:T(8,128)(2,1)S(1)}, bf16[64,2176]{1,0:T(8,128)(2,1)S(1)}, u32[]{:S(2)}, u32[]{:S(2)}) collective-permute-start(bf16[64,2176]{1,0:T(8,128)(2,1)S(1)} %broadcast_multiply_fusion.7), channel_id=1, source_target_pairs={{1,2},{0,63},{3,4},{2,1},{5,6},{4,3},{7,8},{6,5},{9,10},{8,7},{11,... | collective-permute-start | bytes 835592 | tf_op jit(solution)/shard_map/ppermute | solution.py:36
  86.3 7.7 %collective-permute-start.8 = (bf16[64,2176]{1,0:T(8,128)(2,1)S(1)}, bf16[64,2176]{1,0:T(8,128)(2,1)S(1)}, u32[]{:S(2)}, u32[]{:S(2)}) collective-permute-start(bf16[64,2176]{1,0:T(8,128)(2,1)S(1)} %broadcast_multiply_fusion.6), channel_id=1, source_target_pairs={{0,3},{1,62},{2,5},{3,0},{4,7},{5,2},{6,9},{7,4},{8,11},{9,6},{10,... | collective-permute-start | bytes 835592 | tf_op jit(solution)/shard_map/ppermute | solution.py:36
  89.8 8.8 %collective-permute-start.11 = (bf16[64,2176]{1,0:T(8,128)(2,1)S(1)}, bf16[64,2176]{1,0:T(8,128)(2,1)S(1)}, u32[]{:S(2)}, u32[]{:S(2)}) collective-permute-start(bf16[64,2176]{1,0:T(8,128)(2,1)S(1)} %broadcast_multiply_fusion.5), channel_id=1, source_target_pairs={{0,3},{1,62},{2,5},{3,0},{4,7},{5,2},{6,9},{7,4},{8,11},{9,6},{10,... | collective-permute-start | bytes 835592 | tf_op jit(solution)/shard_map/ppermute | solution.py:36
  94.0 11.1 %collective-permute-start.10 = (bf16[64,2176]{1,0:T(8,128)(2,1)S(1)}, bf16[64,2176]{1,0:T(8,128)(2,1)S(1)}, u32[]{:S(2)}, u32[]{:S(2)}) collective-permute-start(bf16[64,2176]{1,0:T(8,128)(2,1)S(1)} %broadcast_multiply_fusion.4), channel_id=1, source_target_pairs={{1,2},{0,63},{3,4},{2,1},{5,6},{4,3},{7,8},{6,5},{9,10},{8,7},{11,... | collective-permute-start | bytes 835592 | tf_op jit(solution)/shard_map/ppermute | solution.py:36
  98.6 12.0 %collective-permute-start.13 = (bf16[64,2176]{1,0:T(8,128)(2,1)S(1)}, bf16[64,2176]{1,0:T(8,128)(2,1)S(1)}, u32[]{:S(2)}, u32[]{:S(2)}) collective-permute-start(bf16[64,2176]{1,0:T(8,128)(2,1)S(1)} %broadcast_multiply_fusion.3), channel_id=1, source_target_pairs={{1,2},{0,63},{3,4},{2,1},{5,6},{4,3},{7,8},{6,5},{9,10},{8,7},{11,... | collective-permute-start | bytes 835592 | tf_op jit(solution)/shard_map/ppermute | solution.py:36
  117.4 8.6 %collective-permute-start.15 = (bf16[64,2176]{1,0:T(8,128)(2,1)S(1)}, bf16[64,2176]{1,0:T(8,128)(2,1)S(1)}, u32[]{:S(2)}, u32[]{:S(2)}) collective-permute-start(bf16[64,2176]{1,0:T(8,128)(2,1)S(1)} %broadcast_multiply_fusion), channel_id=1, source_target_pairs={{0,63},{2,1},{4,3},{6,5},{8,7},{10,9},{12,11},{14,13},{16,15},{18,... | collective-permute-start | bytes 835592 | tf_op jit(solution)/shard_map/ppermute | solution.py:36
  128.8 8.9 %collective-permute-start.20 = (bf16[64,2048]{1,0:T(8,128)(2,1)S(1)}, bf16[64,2048]{1,0:T(8,128)(2,1)S(1)}, u32[]{:S(2)}, u32[]{:S(2)}) collective-permute-start(bf16[64,2048]{1,0:T(8,128)(2,1)S(1)} %get-tuple-element.110), channel_id=1, source_target_pairs={{63,0},{1,2},{3,4},{5,6},{7,8},{9,10},{11,12},{13,14},{15,16},{17,... | collective-permute-start | bytes 786440 | tf_op jit(solution)/shard_map/ppermute | solution.py:36
  130.3 7.6 %collective-permute-start.19 = (bf16[64,2048]{1,0:T(8,128)(2,1)S(1)}, bf16[64,2048]{1,0:T(8,128)(2,1)S(1)}, u32[]{:S(2)}, u32[]{:S(2)}) collective-permute-start(bf16[64,2048]{1,0:T(8,128)(2,1)S(1)} %get-tuple-element.112), channel_id=1, source_target_pairs={{3,0},{62,1},{5,2},{0,3},{7,4},{2,5},{9,6},{4,7},{11,8},{6,9},{13,... | collective-permute-start | bytes 786440 | tf_op jit(solution)/shard_map/ppermute | solution.py:36
  138.0 11.3 %collective-permute-start.21 = (bf16[64,2048]{1,0:T(8,128)(2,1)S(1)}, bf16[64,2048]{1,0:T(8,128)(2,1)S(1)}, u32[]{:S(2)}, u32[]{:S(2)}) collective-permute-start(bf16[64,2048]{1,0:T(8,128)(2,1)S(1)} %add_convert_fusion.12), channel_id=1, source_target_pairs={{2,1},{63,0},{4,3},{1,2},{6,5},{3,4},{8,7},{5,6},{10,9},{7,8},{12,... | collective-permute-start | bytes 786440 | tf_op jit(solution)/shard_map/ppermute | solution.py:36
  143.8 8.9 %collective-permute-start.24 = (bf16[64,2048]{1,0:T(8,128)(2,1)S(1)}, bf16[64,2048]{1,0:T(8,128)(2,1)S(1)}, u32[]{:S(2)}, u32[]{:S(2)}) collective-permute-start(bf16[64,2048]{1,0:T(8,128)(2,1)S(1)} %add_convert_fusion.11), channel_id=1, source_target_pairs={{2,1},{63,0},{4,3},{1,2},{6,5},{3,4},{8,7},{5,6},{10,9},{7,8},{12,... | collective-permute-start | bytes 786440 | tf_op jit(solution)/shard_map/ppermute | solution.py:36
  149.4 7.4 %collective-permute-start.23 = (bf16[64,2048]{1,0:T(8,128)(2,1)S(1)}, bf16[64,2048]{1,0:T(8,128)(2,1)S(1)}, u32[]{:S(2)}, u32[]{:S(2)}) collective-permute-start(bf16[64,2048]{1,0:T(8,128)(2,1)S(1)} %add_convert_fusion.10), channel_id=1, source_target_pairs={{3,0},{62,1},{5,2},{0,3},{7,4},{2,5},{9,6},{4,7},{11,8},{6,9},{13,... | collective-permute-start | bytes 786440 | tf_op jit(solution)/shard_map/ppermute | solution.py:36
  152.7 8.5 %collective-permute-start.26 = (bf16[64,2048]{1,0:T(8,128)(2,1)S(1)}, bf16[64,2048]{1,0:T(8,128)(2,1)S(1)}, u32[]{:S(2)}, u32[]{:S(2)}) collective-permute-start(bf16[64,2048]{1,0:T(8,128)(2,1)S(1)} %add_convert_fusion.9), channel_id=1, source_target_pairs={{3,0},{62,1},{5,2},{0,3},{7,4},{2,5},{9,6},{4,7},{11,8},{6,9},{13,... | collective-permute-start | bytes 786440 | tf_op jit(solution)/shard_map/ppermute | solution.py:36
  156.9 10.7 %collective-permute-start.25 = (bf16[64,2048]{1,0:T(8,128)(2,1)S(1)}, bf16[64,2048]{1,0:T(8,128)(2,1)S(1)}, u32[]{:S(2)}, u32[]{:S(2)}) collective-permute-start(bf16[64,2048]{1,0:T(8,128)(2,1)S(1)} %add_convert_fusion.8), channel_id=1, source_target_pairs={{2,1},{63,0},{4,3},{1,2},{6,5},{3,4},{8,7},{5,6},{10,9},{7,8},{12,... | collective-permute-start | bytes 786440 | tf_op jit(solution)/shard_map/ppermute | solution.py:36
  161.3 9.6 %collective-permute-start.28 = (bf16[64,2048]{1,0:T(8,128)(2,1)S(1)}, bf16[64,2048]{1,0:T(8,128)(2,1)S(1)}, u32[]{:S(2)}, u32[]{:S(2)}) collective-permute-start(bf16[64,2048]{1,0:T(8,128)(2,1)S(1)} %add_convert_fusion.7), channel_id=1, source_target_pairs={{2,1},{63,0},{4,3},{1,2},{6,5},{3,4},{8,7},{5,6},{10,9},{7,8},{12,... | collective-permute-start | bytes 786440 | tf_op jit(solution)/shard_map/ppermute | solution.py:36
  170.9 8.5 %collective-permute-start.30 = (bf16[64,2048]{1,0:T(8,128)(2,1)S(1)}, bf16[64,2048]{1,0:T(8,128)(2,1)S(1)}, u32[]{:S(2)}, u32[]{:S(2)}) collective-permute-start(bf16[64,2048]{1,0:T(8,128)(2,1)S(1)} %add_convert_fusion.5), channel_id=1, source_target_pairs={{3,0},{62,1},{5,2},{0,3},{7,4},{2,5},{9,6},{4,7},{11,8},{6,9},{13,... | collective-permute-start | bytes 786440 | tf_op jit(solution)/shard_map/ppermute | solution.py:36
  174.4 11.2 %collective-permute-start.29 = (bf16[64,2048]{1,0:T(8,128)(2,1)S(1)}, bf16[64,2048]{1,0:T(8,128)(2,1)S(1)}, u32[]{:S(2)}, u32[]{:S(2)}) collective-permute-start(bf16[64,2048]{1,0:T(8,128)(2,1)S(1)} %add_convert_fusion.4), channel_id=1, source_target_pairs={{2,1},{63,0},{4,3},{1,2},{6,5},{3,4},{8,7},{5,6},{10,9},{7,8},{12,... | collective-permute-start | bytes 786440 | tf_op jit(solution)/shard_map/ppermute | solution.py:36
  179.5 9.7 %collective-permute-start.32 = (bf16[64,2048]{1,0:T(8,128)(2,1)S(1)}, bf16[64,2048]{1,0:T(8,128)(2,1)S(1)}, u32[]{:S(2)}, u32[]{:S(2)}) collective-permute-start(bf16[64,2048]{1,0:T(8,128)(2,1)S(1)} %add_convert_fusion.3), channel_id=1, source_target_pairs={{2,1},{63,0},{4,3},{1,2},{6,5},{3,4},{8,7},{5,6},{10,9},{7,8},{12,... | collective-permute-start | bytes 786440 | tf_op jit(solution)/shard_map/ppermute | solution.py:36
  190.0 8.2 %collective-permute-start.33 = (bf16[64,2048]{1,0:T(8,128)(2,1)}, bf16[64,2048]{1,0:T(8,128)(2,1)}, u32[]{:S(2)}, u32[]{:S(2)}) collective-permute-start(bf16[64,2048]{1,0:T(8,128)(2,1)} %add_convert_fusion.1), channel_id=1, source_target_pairs={{3,0},{62,1},{5,2},{0,3},{7,4},{2,5},{9,6},{4,7},{11,8},{6,9},{13,... | collective-permute-start | bytes 786440 | tf_op jit(solution)/shard_map/ppermute | solution.py:36
  192.0 10.7 %collective-permute-start.31 = (bf16[64,2048]{1,0:T(8,128)(2,1)}, bf16[64,2048]{1,0:T(8,128)(2,1)S(1)}, u32[]{:S(2)}, u32[]{:S(2)}) collective-permute-start(bf16[64,2048]{1,0:T(8,128)(2,1)} %add_convert_fusion.2), channel_id=1, source_target_pairs={{3,0},{62,1},{5,2},{0,3},{7,4},{2,5},{9,6},{4,7},{11,8},{6,9},{13,... | collective-permute-start | bytes 786440 | tf_op jit(solution)/shard_map/ppermute | solution.py:36
  199.2 21.1 %collective-permute-start.34 = (bf16[64,2048]{1,0:T(8,128)(2,1)S(1)}, bf16[64,2048]{1,0:T(8,128)(2,1)S(1)}, u32[]{:S(2)}, u32[]{:S(2)}) collective-permute-start(bf16[64,2048]{1,0:T(8,128)(2,1)S(1)} %add_convert_fusion), channel_id=1, source_target_pairs={{16,0},{49,1},{18,2},{51,3},{20,4},{53,5},{22,6},{55,7},{24,8},{57... | collective-permute-start | bytes 786440 | tf_op jit(solution)/shard_map/ppermute | solution.py:36
  220.4 16.7 %collective-permute-start.35 = (bf16[64,1024]{1,0:T(8,128)(2,1)S(1)}, bf16[64,1024]{1,0:T(8,128)(2,1)S(1)}, u32[]{:S(2)}, u32[]{:S(2)}) collective-permute-start(bf16[64,1024]{1,0:T(8,128)(2,1)S(1)} %add_convert_fusion.15), channel_id=1, source_target_pairs={{0,1},{1,0},{2,3},{3,2},{4,5},{5,4},{6,7},{7,6},{8,9},{9,8},{10,11... | collective-permute-start | bytes 393224 | tf_op jit(solution)/shard_map/ppermute | solution.py:160
  (8 other events, 317.0 us)
